TPU v7x, 32 devices: a whole 2x2x4 slice. The times are simulated.
32 devices in a mesh: grp: 2 (over y), ep: 8 (over z, x), tp: 2 (over core).
Axes of the slice: x: 2, y: 2, z: 4, core: 2. Of those that a mesh axis runs over, the one named last changes fastest.
Arguments:
- tokens: bfloat16 [4096, 2048], P(('grp', 'ep', 'tp')), parts along dimension 0, may hold values from -6 to 6
- norm_gain: float32 [2048], replicated, may hold values from 0.1 to 1.9
- expert_ids: int32 [4096, 2], P(('grp', 'ep', 'tp')), parts along dimension 0, may hold values from 0 to 3, all different within a row; in each aligned block of 128 rows (0 to 127, 128 to 255, ...) at most 80 rows name the same one
- route_weights: float32 [4096, 2], P(('grp', 'ep', 'tp')), parts along dimension 0, may hold values from 0.1 to 0.9
- w_gate: bfloat16 [2048, 14336], P(None, ('ep', 'tp')), may hold values from -0.125 to 0.125
- w_up: bfloat16 [2048, 14336], P(None, ('ep', 'tp')), may hold values from -0.125 to 0.125
- w_down: bfloat16 [14336, 2048], P(('ep', 'tp')), may hold values from -0.09375 to 0.09375
Outputs:
- mixed_out: bfloat16 [4096, 2048], P(('grp', 'ep', 'tp')), parts along dimension 0
There are 2 independent parts, one for each index of `grp`. A program takes and returns all parts, laid end to end along the dimension named above; an argument that names none is the same for every part. Nothing has to cross between parts.
Inputs may be any that keep to these rules, and one draw needn't show every extreme that they name: `expert_ids`: each row names 2 different experts. Among the rows of one device no expert is named more than 80 times, and in every draw some expert is named exactly 80 times by one device's rows.
All inputs are finite; a program needn't handle non-finite values.
Results may differ from a plain program's by a relative error of at most 0.01.
Values may be sent and summed in bfloat16 or wider, within the bound.
A program may use at most 128 MiB of HBM per device.

v0:
```python
import jax
import jax.numpy as jnp
from jax import lax
from jax.sharding import PartitionSpec as P


def local(tokens, norm_gain, expert_ids, route_weights, w_gate, w_up, w_down):
    ep_count = lax.axis_size("ep")
    core_count = lax.axis_size("tp")
    expert_count = ep_count // 2
    tok_count = tokens.shape[0]
    model_width = tokens.shape[1]
    top_count = expert_ids.shape[1]
    capacity = 2 * max(1, 5 * tok_count * top_count // (8 * expert_count))
    source = lax.axis_index("ep") * core_count + lax.axis_index("tp")
    values = tokens.astype(jnp.float32)
    scale_rows = lax.rsqrt(jnp.mean(values * values, axis=1, keepdims=True) + 1e-06)
    normed = (values * scale_rows * norm_gain).astype(jnp.bfloat16)
    flat_ids = expert_ids.reshape(-1)
    route_count = flat_ids.shape[0]
    onehot = (flat_ids[:, None] == jnp.arange(expert_count, dtype=jnp.int32)[None, :]).astype(
        jnp.int32
    )
    earlier = jnp.cumsum(onehot, axis=0) - onehot
    slot_base = jnp.sum(earlier * onehot, axis=1)
    slot_index = jnp.remainder(slot_base + source, capacity)
    position = flat_ids * capacity + slot_index
    token_index = jnp.arange(route_count, dtype=jnp.int32) // top_count
    slot_table = (
        jnp.full((expert_count * capacity,), tok_count, jnp.int32).at[position].set(token_index)
    )
    padded = jnp.concatenate([normed, jnp.zeros((1, model_width), jnp.bfloat16)], axis=0)
    buffer = padded[slot_table].reshape(expert_count, capacity, model_width)
    outgoing = jnp.repeat(buffer, 2, axis=0)
    arrived = lax.all_to_all(outgoing, "ep", split_axis=0, concat_axis=0, tiled=True)
    block_rows = lax.all_gather(arrived.reshape(-1, model_width), "tp", axis=0, tiled=True)
    gate_part = jnp.dot(block_rows, w_gate, preferred_element_type=jnp.float32)
    up_part = jnp.dot(block_rows, w_up, preferred_element_type=jnp.float32)
    hidden = (jax.nn.silu(gate_part) * up_part).astype(jnp.bfloat16)
    halves = lax.psum_scatter(
        jnp.dot(hidden, w_down, preferred_element_type=jnp.float32).astype(jnp.bfloat16),
        "tp",
        scatter_dimension=0,
        tiled=True,
    )
    returned = lax.all_to_all(
        halves.reshape(ep_count, capacity, model_width),
        "ep",
        split_axis=0,
        concat_axis=0,
        tiled=True,
    )
    both = jnp.sum(
        returned.reshape(expert_count, 2, capacity, model_width).astype(jnp.float32), axis=1
    )
    summed = lax.optimization_barrier(both.astype(jnp.bfloat16)).astype(jnp.float32)
    picked = summed.reshape(-1, model_width)[position].reshape(tok_count, top_count, model_width)
    mixed_out = jnp.sum(picked * route_weights[:, :, None], axis=1)
    return mixed_out.astype(jnp.bfloat16)


def solution(mesh):
    placed = (
        P(("grp", "ep", "tp"), None),
        P(),
        P(("grp", "ep", "tp"), None),
        P(("grp", "ep", "tp"), None),
        P(None, ("ep", "tp")),
        P(None, ("ep", "tp")),
        P(("ep", "tp"), None),
    )
    return jax.shard_map(
        local, mesh=mesh, in_specs=placed, out_specs=P(("grp", "ep", "tp"), None), check_vma=False
    )
```

profile of v0, /device:TPU:9, one launch (start us, length us, event | category | flops | bytes accessed | tf_op | source)
XLA Modules:
  0.0 219.5 jit_solution(15662699933620368898)
XLA Ops:
  6.5 0.8 copy.12
  7.3 0.1 eq.31
  7.5 0.1 eq.27
  7.6 0.7 broadcast_multiply_fusion
  8.3 1.2 reduce-window.6
  9.5 0.1 slice.12
  9.6 0.1 copy.14
  9.7 0.1 copy.15
  9.8 0.1 add_bitcast_fusion
  9.9 0.1 copy.11
  10.0 0.1 mul.67
  10.2 1.4 scatter_custom_fusion
  11.7 1.2 fusion
  12.9 1.2 fusion.2
  14.2 2.4 %gather_fusion = bf16[320,2048]{1,0:T(8,128)(2,1)S(1)} fusion(bf16[129,2048]{1,0:T(8,128)(2,1)S(1)} %concatenate.3, s32[1024]{0:T(1024)S(1)} %pad_clamp_fusion.1), kind=kCustom, calls=%fused_computation | custom fusion | bytes 2622720 | tf_op jit(solution)/shard_map/gather | solution.py:33
  16.6 0.3 broadcast_in_dim.8
  17.0 63.2 %all_to_all.10 = bf16[8,80,2048]{2,1,0:T(8,128)(2,1)} all-to-all(bf16[8,80,2048]{2,1,0:T(8,128)(2,1)S(1)} %bitcast.36), channel_id=1, replica_groups=mesh['grp'=2,'ep'=8,'tp'=2] {'ep'}, dimensions={0} | all-to-all | bytes 5242880 | tf_op jit(solution)/shard_map/all_to_all | solution.py:35
  80.2 0.0 all-gather.2.cloned.1.call-update
  80.2 0.0 reduce-scatter.2.cloned.1.call-start
  80.3 16.9 %all-gather.2.cloned.1.call-done = bf16[1280,2048]{1,0:T(8,128)(2,1)} async-done(((bf16[640,2048]{1,0:T(8,128)(2,1)}), bf16[1280,2048]{1,0:T(8,128)(2,1)}) %all-gather.2.cloned.1.call-update) | async-done | bytes 5242896 | tf_op jit(solution)/shard_map/all_gather | solution.py:36
  97.2 10.0 %fusion.10 = f32[1280,896]{1,0:T(8,128)} fusion(bf16[1280,2048]{1,0:T(8,128)(2,1)} %all-gather.2.cloned.1.call-done, bf16[2048,896]{1,0:T(8,128)(2,1)} %param.11), kind=kOutput, calls=%fused_computation.36 | convolution fusion | flops 4697620480 | bytes 13500416 | tf_op jit(solution)/shard_map/dot_general | solution.py:37
  107.2 17.6 %convolution_convert_fusion = bf16[1280,2048]{1,0:T(8,128)(2,1)} fusion(bf16[896,2048]{1,0:T(8,128)(2,1)} %param.13, f32[1280,896]{1,0:T(8,128)} %fusion.10, bf16[1280,2048]{1,0:T(8,128)(2,1)} %all-gather.2.cloned.1.call-done, bf16[2048,896]{1,0:T(8,128)(2,1)} %param.12), kind=kOutput, calls=%fused_computation.3 | convolution fusion | flops 9404743680 | bytes 22413312 | tf_op jit(solution)/shard_map/dot_general | solution.py:41
  124.7 0.0 reduce-scatter.2.cloned.1.call-update
  124.8 14.3 %reduce-scatter.2.cloned.1.call-done = bf16[640,2048]{1,0:T(8,128)(2,1)} async-done(((bf16[1280,2048]{1,0:T(8,128)(2,1)}), bf16[640,2048]{1,0:T(8,128)(2,1)}) %reduce-scatter.2.cloned.1.call-update) | async-done | bytes 2621456 | tf_op jit(solution)/shard_map/reduce_scatter | solution.py:40
  139.1 5.5 %all-to-all-start.1 = ((bf16[8,80,2048]{2,1,0:T(8,128)(2,1)}), bf16[8,80,2048]{2,1,0:T(8,128)(2,1)S(1)}, u32[]{:S(2)}, u32[]{:S(2)}) async-start(bf16[8,80,2048]{2,1,0:T(8,128)(2,1)} %bitcast.38), calls=%async_computation.2 | async-start | bytes 5242880 | tf_op jit(solution)/shard_map/all_to_all | solution.py:46
  144.6 0.1 copy.16
  144.7 57.6 %all-to-all-done.1 = bf16[8,80,2048]{2,1,0:T(8,128)(2,1)S(1)} async-done(((bf16[8,80,2048]{2,1,0:T(8,128)(2,1)}), bf16[8,80,2048]{2,1,0:T(8,128)(2,1)S(1)}, u32[]{:S(2)}, u32[]{:S(2)}) %all-to-all-start.1) | async-done | bytes 2621472 | tf_op jit(solution)/shard_map/all_to_all | solution.py:46
  202.3 0.7 bitcast_reduce_fusion
  203.0 0.4 bitcast_convert_fusion
  203.4 2.7 %gather_fusion.1 = f32[256,2048]{1,0:T(8,128)} fusion(f32[320,2048]{1,0:T(8,128)S(1)} %bitcast_convert_fusion, s32[1024]{0:T(1024)S(1)} %pad_clamp_fusion), kind=kCustom, calls=%fused_computation.1 | custom fusion | bytes 4195328 | tf_op jit(solution)/shard_map/gather | solution.py:57
  206.1 2.5 %reshape.113 = f32[128,2,2048]{2,1,0:T(2,128)S(1)} reshape(f32[256,2048]{1,0:T(8,128)} %gather_fusion.1) | data formatting | bytes 4194304 | tf_op jit(solution)/shard_map/reshape | solution.py:57
  208.6 4.0 %multiply_reduce_fusion = bf16[128,2048]{1,0:T(8,128)(2,1)} fusion(f32[128,2,2048]{2,1,0:T(2,128)S(1)} %reshape.113, f32[128,2]{1,0:T(8,128)S(1)} %copy.16), kind=kLoop, calls=%fused_computation.6 | loop fusion | flops 786432 | bytes 2622464 | tf_op jit(solution)/shard_map/reduce_sum | solution.py:58
  (15 shorter events, 0.2 us)
Async XLA Ops:
  6.5 90.7 %all-gather.2.cloned.1.call-start = ((), (), s32[]{:S(2)}) async-start(), calls=%async_computation.3 | async-start | bytes 7864320 | tf_op jit(solution)/shard_map/all_gather | solution.py:36
  80.2 58.9 %reduce-scatter.2.cloned.1.call-start = ((), (), s32[]{:S(2)}) async-start(), calls=%async_computation.4 | async-start | bytes 7864320 | tf_op jit(solution)/shard_map/reduce_scatter | solution.py:40
  124.8 19.8 %copy-start = (f32[128,2]{0,1:T(2,128)S(1)}, f32[128,2]{0,1:T(2,128)}, u32[]{:S(2)}) copy-start(f32[128,2]{0,1:T(2,128)} %param.10) | copy-start | bytes 3076
  139.1 63.2 %all-to-all-start.1 = ((bf16[8,80,2048]{2,1,0:T(8,128)(2,1)}), bf16[8,80,2048]{2,1,0:T(8,128)(2,1)S(1)}, u32[]{:S(2)}, u32[]{:S(2)}) async-start(bf16[8,80,2048]{2,1,0:T(8,128)(2,1)} %bitcast.38), calls=%async_computation.2 | async-start | bytes 5242880 | tf_op jit(solution)/shard_map/all_to_all | solution.py:46
Sparse Core Ops, SparseCore 0:
  80.3 16.8 all-gather.1
  124.9 14.1 reduce-scatter.1
where the time goes:
time: 223 us; the launch traced here: 219 us
  waiting for transfers between devices  88.9 us (40%)
  blocking collectives  63.2 us (28%)
  matrix products  27.5 us (12%)
  between operations  13.5 us (6%)
  local copies, waits for them, and re-layouts  11.1 us (5%)
  other arithmetic  9.64 us (4%)
  starting transfers between devices  5.53 us (2%)
    all_to_all x1, blocking collectives, local(): lax.all_to_all(outgoing, 'ep', split_axis=0, concat_axis=0, tiled=True)  63.2 us
    all_to_all x1, waiting for transfers between devices, local(): lax.all_to_all(halves.reshape(ep_count, capacity, model_width), 'ep', spl...  57.6 us
    dot_general x1, matrix products, local(): jnp.dot(hidden, w_down, preferred_element_type=jnp.float32)  17.6 us
    all_gather x1, waiting for transfers between devices, local(): lax.all_gather(arrived.reshape(-1, model_width), 'tp', axis=0, tiled=True)  16.9 us
    reduce_scatter x1, waiting for transfers between devices, local(): lax.psum_scatter(jnp.dot(hidden, w_down, preferred_element_type=jnp.float...  14.3 us
    dot_general x1, matrix products, local(): gate_part = jnp.dot(block_rows, w_gate, preferred_element_type=jnp.float32)  9.98 us
    all_to_all x1, starting transfers between devices, local(): lax.all_to_all(halves.reshape(ep_count, capacity, model_width), 'ep', spl...  5.48 us
  transfers between devices with their start and end apart: 3, of which 3 were waited for; matrix products, arithmetic and copies ran while one was open for 0% of the time, Pallas kernels for 0%

commit v1 on v0

v1 whole, which is shorter than its diff:
```python
import functools

import jax
import jax.numpy as jnp
from jax import lax
from jax.experimental import pallas as pl
from jax.experimental.pallas import tpu as pltpu
from jax.sharding import PartitionSpec as P

MESH = pl.DeviceIdType.MESH
LANE = 128


def mix_index(first, second, count):
    total = first * 0
    bit = 1
    while bit < count:
        one, two = (first // bit) % 2, (second // bit) % 2
        total = total + bit * (one + two - 2 * one * two)
        bit *= 2
    return total


def kernel(
    experts, cap,
    tok_ref, gain_ref, ids_ref, ids_t_ref, weight_ref, gate_ref, up_ref, down_ref,
    out_ref,
    norm, xs, xa, hid, po, rd, cx, rx, fo, ret, wgu, wd,
    gate_sem, up_sem, down_sem, own_sem,
    z_send, z_recv, x_send, x_recv, d_send, d_recv, e_send, e_recv,
    r_send, r_recv, v_send, v_recv, w_send, w_recv,
):
    ep, c = lax.axis_index("ep"), lax.axis_index("tp")
    p, h = ep // 2, ep % 2
    toks, width = tok_ref.shape
    tiles = wgu.shape[0]
    across = {"ep": 2 * p + 1 - h, "tp": c}
    beside = {"ep": ep, "tp": 1 - c}

    def plane(q):
        return {"ep": 2 * q + h, "tp": c}

    barrier = pltpu.get_barrier_semaphore()

    def greet(k, carry):
        pl.semaphore_signal(barrier, inc=1, device_id=plane(mix_index(p, k, experts)), device_id_type=MESH)
        return carry

    lax.fori_loop(1, experts, greet, 0)
    pl.semaphore_signal(barrier, inc=1, device_id=across, device_id_type=MESH)
    pl.semaphore_signal(barrier, inc=1, device_id=beside, device_id_type=MESH)

    def gate_copy(j):
        return pltpu.make_async_copy(
            gate_ref.at[:, pl.ds(j * LANE, LANE)], wgu.at[j, :, pl.ds(0, LANE)], gate_sem.at[j])

    def up_copy(j):
        return pltpu.make_async_copy(
            up_ref.at[:, pl.ds(j * LANE, LANE)], wgu.at[j, :, pl.ds(LANE, LANE)], up_sem.at[j])

    down_copy = pltpu.make_async_copy(down_ref, wd, down_sem)
    for j in range(tiles):
        gate_copy(j).start()
        up_copy(j).start()
    down_copy.start()

    values = tok_ref[...].astype(jnp.float32)
    scale_rows = lax.rsqrt(jnp.mean(values * values, axis=1, keepdims=True) + 1e-06)
    norm[...] = (values * scale_rows * gain_ref[...]).astype(jnp.bfloat16)

    row = lax.broadcasted_iota(jnp.int32, (toks, toks), 0)
    col = lax.broadcasted_iota(jnp.int32, (toks, toks), 1)
    before = (row < col).astype(jnp.float32).astype(jnp.bfloat16)
    slots = lax.broadcasted_iota(jnp.int32, (cap, toks), 0).astype(jnp.float32)

    def fill(e, carry):
        named = ((ids_t_ref[0:1, :] == e) | (ids_t_ref[1:2, :] == e)).astype(jnp.float32)
        rank = jnp.dot(
            jnp.broadcast_to(named, (16, toks)).astype(jnp.bfloat16), before,
            preferred_element_type=jnp.float32)[0:1, :]
        pick = jnp.where(slots == rank, named, 0.0).astype(jnp.bfloat16)
        xs[e] = jnp.dot(pick, norm[...], preferred_element_type=jnp.float32).astype(jnp.bfloat16)
        return carry

    lax.fori_loop(0, experts, fill, 0)
    pl.semaphore_wait(barrier, experts + 1)

    def remote(src, dst, send, recv, target):
        return pltpu.make_async_remote_copy(
            src_ref=src, dst_ref=dst, send_sem=send, recv_sem=recv, device_id=target, device_id_type=MESH)

    def z_copy(k):
        q = mix_index(p, k, experts)
        return remote(xs.at[q], xa.at[4 * p + 2 * h + c], z_send.at[k], z_recv.at[k], plane(q))

    def z_land(k):
        q = mix_index(p, k, experts)
        return remote(xs.at[q], xa.at[4 * q + 2 * h + c], z_send.at[k], z_recv.at[k], plane(q))

    own_copy = pltpu.make_async_copy(xs.at[p], xa.at[4 * p + 2 * h + c], own_sem)

    def mine(k, half, core):
        return xa.at[4 * mix_index(p, k, experts) + 2 * half + core]

    def x_copy(k):
        return remote(mine(k, h, c), mine(k, h, c), x_send.at[k], x_recv.at[k], across)

    def x_land(k):
        return remote(mine(k, h, c), mine(k, 1 - h, c), x_send.at[k], x_recv.at[k], across)

    def d_copy(k):
        return remote(mine(k, h, c), mine(k, h, c), d_send.at[k], d_recv.at[k], beside)

    def d_land(k):
        return remote(mine(k, h, c), mine(k, h, 1 - c), d_send.at[k], d_recv.at[k], beside)

    def e_copy(k):
        return remote(mine(k, 1 - h, c), mine(k, 1 - h, c), e_send.at[k], e_recv.at[k], beside)

    def e_land(k):
        return remote(mine(k, 1 - h, c), mine(k, 1 - h, 1 - c), e_send.at[k], e_recv.at[k], beside)

    def r_copy(k, half):
        return remote(
            po.at[4 * k + 2 * half + 1 - c], rd.at[2 * k + half],
            r_send.at[2 * k + half], r_recv.at[2 * k + half], beside)

    def v_copy(k):
        return remote(cx.at[2 * k + 1 - h], rx.at[k], v_send.at[k], v_recv.at[k], across)

    def w_copy(k):
        return remote(fo.at[k], ret.at[p], w_send.at[k], w_recv.at[k], plane(mix_index(p, k, experts)))

    def w_land(k):
        q = mix_index(p, k, experts)
        return remote(fo.at[k], ret.at[q], w_send.at[k], w_recv.at[k], plane(q))

    own_copy.start()

    def send(k, carry):
        z_copy(k).start()
        return carry

    lax.fori_loop(1, experts, send, 0)
    own_copy.wait()

    def compute(k):
        first = 4 * mix_index(p, k, experts)

        def gate_up(j, carry):
            rows = xa[pl.ds(first, 4)].reshape(4 * cap, width)
            both = jnp.dot(rows, wgu[j], preferred_element_type=jnp.float32)
            gate, up = both[:, :LANE], both[:, LANE:]
            hid[:, pl.ds(pl.multiple_of(j * LANE, LANE), LANE)] = (
                gate / (1.0 + jnp.exp(-gate)) * up).astype(jnp.bfloat16)
            return carry

        lax.fori_loop(0, tiles, gate_up, 0)
        step = 2 * LANE

        def down(n, carry):
            place = pl.ds(pl.multiple_of(n * step, step), step)
            part = jnp.dot(hid[...], wd[:, place], preferred_element_type=jnp.float32)
            po[pl.ds(4 * k, 4), :, place] = part.astype(jnp.bfloat16).reshape(4, cap, step)
            return carry

        lax.fori_loop(0, width // step, down, 0)

    def finish(k):
        v_copy(k).wait_recv()
        total = (cx[2 * k + h].astype(jnp.float32) + rx[k].astype(jnp.float32)).astype(jnp.bfloat16)

        @pl.when(k == 0)
        def _():
            ret[p] = total

        @pl.when(k > 0)
        def _():
            fo[k] = total
            w_copy(k).start()

    def stage(i, carry):
        @pl.when(i < experts)
        def _():
            @pl.when(i > 0)
            def _():
                z_land(i).wait_recv()

            x_copy(i).start()
            d_copy(i).start()

        @pl.when(i > 0)
        def _():
            k = i - 1
            x_land(k).wait_recv()
            e_copy(k).start()

            @pl.when(k == 0)
            def _():
                for j in range(tiles):
                    gate_copy(j).wait()
                    up_copy(j).wait()
                down_copy.wait()

            d_land(k).wait_recv()
            e_land(k).wait_recv()
            compute(k)
            for half in range(2):
                r_copy(k, half).start()

            @pl.when(k > 0)
            def _():
                finish(k - 1)

            for half in range(2):
                r_copy(k, half).wait_recv()
                cx[2 * k + half] = (
                    po[4 * k + 2 * half + c].astype(jnp.float32) + rd[2 * k + half].astype(jnp.float32)
                ).astype(jnp.bfloat16)
            v_copy(k).start()

        return carry

    lax.fori_loop(0, experts + 1, stage, 0)
    finish(experts - 1)

    def settle(k, carry):
        x_copy(k).wait_send()
        d_copy(k).wait_send()
        e_copy(k).wait_send()
        r_copy(k, 0).wait_send()
        r_copy(k, 1).wait_send()
        v_copy(k).wait_send()

        @pl.when(k > 0)
        def _():
            z_copy(k).wait_send()
            w_copy(k).wait_send()
            w_land(k).wait_recv()

        return carry

    after = (col < row).astype(jnp.float32).astype(jnp.bfloat16)

    def place_of(e, places):
        hits = [(ids_ref[:, n:n + 1] == e).astype(jnp.float32) for n in range(2)]
        rank = jnp.dot(
            after, jnp.broadcast_to(hits[0] + hits[1], (toks, LANE)).astype(jnp.bfloat16),
            preferred_element_type=jnp.float32)[:, 0:1]
        spot = rank + lax.convert_element_type(e * cap, jnp.float32)
        return tuple(old + hit * spot for old, hit in zip(places, hits))

    zero = jnp.zeros((toks, 1), jnp.float32)
    places = lax.fori_loop(0, experts, place_of, (zero, zero))
    lax.fori_loop(0, experts, settle, 0)
    lanes = lax.broadcasted_iota(jnp.int32, (toks, experts * cap), 1).astype(jnp.float32)
    picks = [(lanes == place).astype(jnp.float32).astype(jnp.bfloat16) for place in places]
    step = 4 * LANE
    for n in range(width // step):
        cut = pl.ds(n * step, step)
        rows = ret[:, :, cut].reshape(experts * cap, step)
        total = jnp.zeros((toks, step), jnp.float32)
        for m in range(2):
            total = total + weight_ref[:, m:m + 1] * jnp.dot(
                picks[m], rows, preferred_element_type=jnp.float32)
        out_ref[:, cut] = total.astype(jnp.bfloat16)


def local(tokens, norm_gain, expert_ids, route_weights, w_gate, w_up, w_down):
    experts = lax.axis_size("ep") // 2
    toks, width = tokens.shape
    hidden = w_gate.shape[1]
    capacity = 2 * max(1, 5 * toks * expert_ids.shape[1] // (8 * experts))
    cap = -(-capacity // 16) * 16
    tiles = hidden // LANE
    vmem, any_space = pl.BlockSpec(memory_space=pltpu.VMEM), pl.BlockSpec(memory_space=pl.ANY)
    dma = pltpu.SemaphoreType.DMA
    bf16 = jnp.bfloat16
    return pl.pallas_call(
        functools.partial(kernel, experts, cap),
        out_shape=jax.ShapeDtypeStruct((toks, width), bf16),
        in_specs=[vmem] * 5 + [any_space] * 3,
        out_specs=vmem,
        scratch_shapes=[
            pltpu.VMEM((toks, width), bf16),
            pltpu.VMEM((experts, cap, width), bf16),
            pltpu.VMEM((experts * 4, cap, width), bf16),
            pltpu.VMEM((4 * cap, hidden), bf16),
            pltpu.VMEM((experts * 4, cap, width), bf16),
            pltpu.VMEM((experts * 2, cap, width), bf16),
            pltpu.VMEM((experts * 2, cap, width), bf16),
            pltpu.VMEM((experts, cap, width), bf16),
            pltpu.VMEM((experts, cap, width), bf16),
            pltpu.VMEM((experts, cap, width), bf16),
            pltpu.VMEM((tiles, width, 2 * LANE), bf16),
            pltpu.VMEM((hidden, width), bf16),
            dma((tiles,)), dma((tiles,)), dma, dma,
        ] + [dma((experts,))] * 8 + [dma((2 * experts,))] * 2 + [dma((experts,))] * 4,
        compiler_params=pltpu.CompilerParams(
            collective_id=0, has_side_effects=True, vmem_limit_bytes=60 * 1024 * 1024),
    )(tokens, norm_gain.reshape(1, -1), expert_ids, expert_ids.T, route_weights, w_gate, w_up, w_down)


def solution(mesh):
    placed = (
        P(("grp", "ep", "tp"), None),
        P(),
        P(("grp", "ep", "tp"), None),
        P(("grp", "ep", "tp"), None),
        P(None, ("ep", "tp")),
        P(None, ("ep", "tp")),
        P(("ep", "tp"), None),
    )
    return jax.shard_map(
        local, mesh=mesh, in_specs=placed, out_specs=P(("grp", "ep", "tp"), None), check_vma=False
    )
```

time: 223 us -> 99 us (0.44); the launches traced: 219 us -> 98.8 us
  Pallas kernels: 0 us -> 94.1 us
  waiting for transfers between devices: 88.9 us -> 0 us
  blocking collectives: 63.2 us -> 0 us
  matrix products: 27.5 us -> 0 us
  between operations: 13.5 us -> 0.01 us
  other arithmetic: 9.64 us -> 0 us
  local copies, waits for them, and re-layouts: 11.1 us -> 4.7 us
  starting transfers between devices: 5.53 us -> 0 us
    pallas_call x0 -> x1, Pallas kernels: none -> 94.1 us  [local(): pl.pallas_call(functools.partial(kernel, experts, cap), out_shape=jax.Sha...]
    all_to_all x1 -> x0, blocking collectives: 63.2 us -> none  [local(): lax.all_to_all(outgoing, 'ep', split_axis=0, concat_axis=0, tiled=True)]
    all_to_all x1 -> x0, waiting for transfers between devices: 57.6 us -> none  [local(): lax.all_to_all(halves.reshape(ep_count, capacity, model_width), 'ep', spl...]
    dot_general x2 -> x0, matrix products: 27.5 us -> none  [the longest x1 17.6 us: local(): jnp.dot(hidden, w_down, preferred_element_type=jnp.float32)]
    all_gather x1 -> x0, waiting for transfers between devices: 16.9 us -> none  [local(): lax.all_gather(arrived.reshape(-1, model_width), 'tp', axis=0, tiled=True)]
    reduce_scatter x1 -> x0, waiting for transfers between devices: 14.3 us -> none  [local(): lax.psum_scatter(jnp.dot(hidden, w_down, preferred_element_type=jnp.float...]
    reduce_sum x4 -> x0, other arithmetic: 5.94 us -> none  [the longest x1 4.03 us: local(): mixed_out = jnp.sum(picked * route_weights[:, :, None], axis=1)]
    all_to_all x1 -> x0, starting transfers between devices: 5.48 us -> none  [local(): lax.all_to_all(halves.reshape(ep_count, capacity, model_width), 'ep', spl...]
  transfers between devices with their start and end apart: 3 -> 0, of which waited for: 3 -> 0; matrix products, arithmetic and copies ran while one was open for 0% -> 0% of each run, Pallas kernels for 0% -> 0%
where the time goes in v1:
time: 99 us; the launch traced here: 98.8 us
  Pallas kernels  94.1 us (95%)
  local copies, waits for them, and re-layouts  4.7 us (5%)
    pallas_call x1, Pallas kernels, local(): pl.pallas_call(functools.partial(kernel, experts, cap), out_shape=jax.Sha...  94.1 us
    unnamed x3, local copies, waits for them, and re-layouts  4.7 us

profile of v1, /device:TPU:9, one launch (start us, length us, event | category | flops | bytes accessed | tf_op | source)
XLA Modules:
  0.0 98.8 jit_solution(14887381703232014876)
XLA Ops:
  0.0 1.4 %copy.9.weight_ref = f32[128,2]{1,0:T(8,128)} copy(f32[128,2]{0,1:T(2,128)} %param.10) | data formatting | bytes 2048 | tf_op args[3]
  1.4 1.4 %copy.8.ids_ref = s32[128,2]{1,0:T(8,128)} copy(s32[128,2]{0,1:T(2,128)} %param.9) | data formatting | bytes 2048 | tf_op args[2]
  2.8 94.1 %shard_map.73 = bf16[128,2048]{1,0:T(8,128)(2,1)} custom-call(bf16[128,2048]{1,0:T(8,128)(2,1)} %tok_ref.1, f32[1,2048]{1,0:T(1,128)} %bitcast.2, s32[128,2]{1,0:T(8,128)} %copy.8.ids_ref, s32[2,128]{1,0:T(2,128)} %bitcast.3, f32[128,2]{1,0:T(8,128)} %copy.9.weight_ref, bf16[2048,896]{1,0:T(8,128)(2,1)} %gate_ref.1, bf16[2048,896]{1,0:T(8,128)(2,1)} %up_ref.1, ...), custom_call_target="tpu_custom_call" | custom-call | tf_op jit(solution)/shard_map/pallas_call | solution.py:279
  96.9 1.9 %copy.11 = bf16[128,2048]{1,0:T(8,128)(2,1)} copy(bf16[128,2048]{1,0:T(8,128)(2,1)} %shard_map.73) | data formatting | bytes 1048576

commit v2 on v1

v2 whole, which is shorter than its diff:
```python
import functools

import jax
import jax.numpy as jnp
from jax import lax
from jax.experimental import pallas as pl
from jax.experimental.pallas import tpu as pltpu
from jax.sharding import PartitionSpec as P

MESH = pl.DeviceIdType.MESH
LANE = 128
PIECES = 2


def turn(i, experts):
    return i % experts


def mix_index(first, second, count):
    total = first * 0
    bit = 1
    while bit < count:
        one, two = (first // bit) % 2, (second // bit) % 2
        total = total + bit * (one + two - 2 * one * two)
        bit *= 2
    return total


def kernel(
    experts, cap,
    tok_ref, gain_ref, ids_ref, weight_ref, gate_ref, up_ref, down_ref,
    out_ref,
    norm, xs, xa, hid, po, rd, cx, rx, fo, ret, wgu, wd,
    gate_sem, up_sem, down_sem, own_sem,
    z_send, z_recv, x_send, x_recv, d_send, d_recv, e_send, e_recv,
    r_send, r_recv, v_send, v_recv, w_send, w_recv,
):
    ep, c = lax.axis_index("ep"), lax.axis_index("tp")
    p, h = ep // 2, ep % 2
    toks, width = tok_ref.shape
    tiles = wgu.shape[0]
    part_width = width // PIECES
    across = {"ep": 2 * p + 1 - h, "tp": c}
    beside = {"ep": ep, "tp": 1 - c}

    def plane(q):
        return {"ep": 2 * q + h, "tp": c}

    barrier = pltpu.get_barrier_semaphore()

    def greet(k, carry):
        pl.semaphore_signal(barrier, inc=1, device_id=plane(mix_index(p, k, experts)), device_id_type=MESH)
        return carry

    lax.fori_loop(1, experts, greet, 0)
    pl.semaphore_signal(barrier, inc=1, device_id=across, device_id_type=MESH)
    pl.semaphore_signal(barrier, inc=1, device_id=beside, device_id_type=MESH)

    def gate_copy(j):
        return pltpu.make_async_copy(
            gate_ref.at[:, pl.ds(j * LANE, LANE)], wgu.at[j, :, pl.ds(0, LANE)], gate_sem.at[j])

    def up_copy(j):
        return pltpu.make_async_copy(
            up_ref.at[:, pl.ds(j * LANE, LANE)], wgu.at[j, :, pl.ds(LANE, LANE)], up_sem.at[j])

    down_copy = pltpu.make_async_copy(down_ref, wd, down_sem)
    for j in range(tiles):
        gate_copy(j).start()
        up_copy(j).start()
    down_copy.start()

    values = tok_ref[...].astype(jnp.float32)
    scale_rows = lax.rsqrt(jnp.mean(values * values, axis=1, keepdims=True) + 1e-06)
    norm[...] = (values * scale_rows * gain_ref[...]).astype(jnp.bfloat16)

    row = lax.broadcasted_iota(jnp.int32, (toks, toks), 0)
    col = lax.broadcasted_iota(jnp.int32, (toks, toks), 1)
    before = (row < col).astype(jnp.float32).astype(jnp.bfloat16)
    slots = lax.broadcasted_iota(jnp.int32, (cap, toks), 0).astype(jnp.float32)

    def remote(src, dst, send, recv, target):
        return pltpu.make_async_remote_copy(
            src_ref=src, dst_ref=dst, send_sem=send, recv_sem=recv, device_id=target, device_id_type=MESH)

    def cut(ref, index, g):
        return ref.at[index, :, pl.ds(g * part_width, part_width)]

    def z_pair(k, g, origin):
        q = mix_index(p, k, experts)
        n = PIECES * k + g
        return remote(
            cut(xs, q, g), cut(xa, 4 * origin(q) + 2 * h + c, g), z_send.at[n], z_recv.at[n], plane(q))

    def z_copy(k, g):
        return z_pair(k, g, lambda q: p)

    def z_land(k, g):
        return z_pair(k, g, lambda q: q)

    own_copy = pltpu.make_async_copy(xs.at[p], xa.at[4 * p + 2 * h + c], own_sem)

    def mine(k, half, core, g):
        return cut(xa, 4 * mix_index(p, k, experts) + 2 * half + core, g)

    def shift(k, g, there, here, send, recv, target):
        n = PIECES * k + g
        return remote(mine(k, *there, g), mine(k, *here, g), send.at[n], recv.at[n], target)

    def x_copy(k, g):
        return shift(k, g, (h, c), (h, c), x_send, x_recv, across)

    def x_land(k, g):
        return shift(k, g, (h, c), (1 - h, c), x_send, x_recv, across)

    def d_copy(k, g):
        return shift(k, g, (h, c), (h, c), d_send, d_recv, beside)

    def d_land(k, g):
        return shift(k, g, (h, c), (h, 1 - c), d_send, d_recv, beside)

    def e_copy(k, g):
        return shift(k, g, (1 - h, c), (1 - h, c), e_send, e_recv, beside)

    def e_land(k, g):
        return shift(k, g, (1 - h, c), (1 - h, 1 - c), e_send, e_recv, beside)

    def r_copy(k, half, g):
        n = 2 * (PIECES * k + g) + half
        return remote(
            cut(po, 4 * k + 2 * half + 1 - c, g), cut(rd, 2 * k + half, g),
            r_send.at[n], r_recv.at[n], beside)

    def v_copy(k, g):
        n = PIECES * k + g
        return remote(cut(cx, 2 * k + 1 - h, g), cut(rx, k, g), v_send.at[n], v_recv.at[n], across)

    def w_pair(k, g, origin):
        q = mix_index(p, k, experts)
        n = PIECES * k + g
        return remote(cut(fo, k, g), cut(ret, origin(q), g), w_send.at[n], w_recv.at[n], plane(q))

    def w_copy(k, g):
        return w_pair(k, g, lambda q: p)

    def w_land(k, g):
        return w_pair(k, g, lambda q: q)

    pl.semaphore_wait(barrier, experts + 1)

    def fill(i, carry):
        k = turn(i + 1, experts)
        e = mix_index(p, k, experts)
        named = ((ids_ref[0:1, :] == e) | (ids_ref[1:2, :] == e)).astype(jnp.float32)
        rank = jnp.dot(
            jnp.broadcast_to(named, (16, toks)).astype(jnp.bfloat16), before,
            preferred_element_type=jnp.float32)[0:1, :]
        pick = jnp.where(slots == rank, named, 0.0).astype(jnp.bfloat16)
        xs[e] = jnp.dot(pick, norm[...], preferred_element_type=jnp.float32).astype(jnp.bfloat16)

        @pl.when(k > 0)
        def _():
            for g in range(PIECES):
                z_copy(k, g).start()

        return carry

    lax.fori_loop(0, experts, fill, 0)
    own_copy.start()
    own_copy.wait()

    step = 2 * LANE

    def compute(k):
        first = 4 * mix_index(p, k, experts)

        def gate_up(j, carry):
            rows = xa[pl.ds(first, 4)].reshape(4 * cap, width)
            both = jnp.dot(rows, wgu[j], preferred_element_type=jnp.float32)
            gate, up = both[:, :LANE], both[:, LANE:]
            hid[:, pl.ds(pl.multiple_of(j * LANE, LANE), LANE)] = (
                gate / (1.0 + jnp.exp(-gate)) * up).astype(jnp.bfloat16)
            return carry

        lax.fori_loop(0, tiles, gate_up, 0)

        def down(n, carry):
            place = pl.ds(pl.multiple_of(n * step, step), step)
            part = jnp.dot(hid[...], wd[:, place], preferred_element_type=jnp.float32)
            po[pl.ds(4 * k, 4), :, place] = part.astype(jnp.bfloat16).reshape(4, cap, step)
            return carry

        many = part_width // step
        for g in range(PIECES):
            lax.fori_loop(g * many, (g + 1) * many, down, 0)
            for half in range(2):
                r_copy(k, half, g).start()

    def add(first, second):
        return (first.astype(jnp.float32) + second.astype(jnp.float32)).astype(jnp.bfloat16)

    def finish(k):
        for g in range(PIECES):
            v_copy(k, g).wait_recv()
            cols = pl.ds(g * part_width, part_width)
            total = add(cx[2 * k + h, :, cols], rx[k, :, cols])

            @pl.when(k == 0)
            def _():
                ret[p, :, cols] = total

            @pl.when(k > 0)
            def _():
                fo[k, :, cols] = total
                w_copy(k, g).start()

    def stage(i, carry):
        @pl.when(i < experts)
        def _():
            k = turn(i, experts)
            for g in range(PIECES):
                @pl.when(k > 0)
                def _():
                    z_land(k, g).wait_recv()

                x_copy(k, g).start()
                d_copy(k, g).start()

        @pl.when(i > 0)
        def _():
            k = turn(i - 1, experts)
            for g in range(PIECES):
                x_land(k, g).wait_recv()
                e_copy(k, g).start()

            @pl.when(i == 1)
            def _():
                for j in range(tiles):
                    gate_copy(j).wait()
                    up_copy(j).wait()
                down_copy.wait()

            for g in range(PIECES):
                d_land(k, g).wait_recv()
                e_land(k, g).wait_recv()
            compute(k)

            @pl.when(i > 2)
            def _():
                finish(turn(i - 2, experts))

            for g in range(PIECES):
                cols = pl.ds(g * part_width, part_width)
                for half in range(2):
                    r_copy(k, half, g).wait_recv()
                    cx[2 * k + half, :, cols] = add(
                        po[4 * k + 2 * half + c, :, cols], rd[2 * k + half, :, cols])

                @pl.when(k > 0)
                def _():
                    v_copy(k, g).start()

        return carry

    lax.fori_loop(0, experts + 1, stage, 0)
    for g in range(PIECES):
        v_copy(0, g).start()

    def settle(k, carry):
        for g in range(PIECES):
            x_copy(k, g).wait_send()
            d_copy(k, g).wait_send()
            e_copy(k, g).wait_send()
            r_copy(k, 0, g).wait_send()
            r_copy(k, 1, g).wait_send()
            v_copy(k, g).wait_send()

            @pl.when(k > 0)
            def _():
                z_copy(k, g).wait_send()
                w_copy(k, g).wait_send()

        return carry

    after = (col < row).astype(jnp.float32).astype(jnp.bfloat16)

    sides = jnp.concatenate(
        [ids_ref[...].astype(jnp.float32), weight_ref[...], jnp.zeros((LANE - 4, toks), jnp.float32)], axis=0).T

    def place_of(e, places):
        number = lax.convert_element_type(e, jnp.float32)
        hits = [(sides[:, n:n + 1] == number).astype(jnp.float32) for n in range(2)]
        rank = jnp.dot(
            after, jnp.broadcast_to(hits[0] + hits[1], (toks, LANE)).astype(jnp.bfloat16),
            preferred_element_type=jnp.float32)[:, 0:1]
        spot = rank + number * cap
        return tuple(old + hit * spot for old, hit in zip(places, hits))

    zero = jnp.zeros((toks, 1), jnp.float32)
    places = lax.fori_loop(0, experts, place_of, (zero, zero))
    lanes = lax.broadcasted_iota(jnp.int32, (toks, experts * cap), 1).astype(jnp.float32)
    picks = [(lanes == place).astype(jnp.float32).astype(jnp.bfloat16) for place in places]
    finish(turn(experts - 1, experts))
    finish(0)
    lax.fori_loop(0, experts, settle, 0)
    for g in range(PIECES):
        def landed(k, carry):
            w_land(k, g).wait_recv()
            return carry

        lax.fori_loop(1, experts, landed, 0)
        cols = pl.ds(g * part_width, part_width)
        rows = ret[:, :, cols].reshape(experts * cap, part_width)
        total = jnp.zeros((toks, part_width), jnp.float32)
        for m in range(2):
            total = total + sides[:, 2 + m:3 + m] * jnp.dot(
                picks[m], rows, preferred_element_type=jnp.float32)
        out_ref[:, cols] = total.astype(jnp.bfloat16)


def local(tokens, norm_gain, expert_ids, route_weights, w_gate, w_up, w_down):
    experts = lax.axis_size("ep") // 2
    toks, width = tokens.shape
    hidden = w_gate.shape[1]
    capacity = 2 * max(1, 5 * toks * expert_ids.shape[1] // (8 * experts))
    cap = -(-capacity // 16) * 16
    tiles = hidden // LANE
    vmem, any_space = pl.BlockSpec(memory_space=pltpu.VMEM), pl.BlockSpec(memory_space=pl.ANY)
    dma = pltpu.SemaphoreType.DMA
    bf16 = jnp.bfloat16
    return pl.pallas_call(
        functools.partial(kernel, experts, cap),
        out_shape=jax.ShapeDtypeStruct((toks, width), bf16),
        in_specs=[vmem] * 4 + [any_space] * 3,
        out_specs=vmem,
        scratch_shapes=[
            pltpu.VMEM((toks, width), bf16),
            pltpu.VMEM((experts, cap, width), bf16),
            pltpu.VMEM((experts * 4, cap, width), bf16),
            pltpu.VMEM((4 * cap, hidden), bf16),
            pltpu.VMEM((experts * 4, cap, width), bf16),
            pltpu.VMEM((experts * 2, cap, width), bf16),
            pltpu.VMEM((experts * 2, cap, width), bf16),
            pltpu.VMEM((experts, cap, width), bf16),
            pltpu.VMEM((experts, cap, width), bf16),
            pltpu.VMEM((experts, cap, width), bf16),
            pltpu.VMEM((tiles, width, 2 * LANE), bf16),
            pltpu.VMEM((hidden, width), bf16),
            dma((tiles,)), dma((tiles,)), dma, dma,
        ] + [dma((PIECES * experts,))] * 8 + [dma((2 * PIECES * experts,))] * 2 + [dma((PIECES * experts,))] * 4,
        compiler_params=pltpu.CompilerParams(
            collective_id=0, has_side_effects=True, vmem_limit_bytes=60 * 1024 * 1024),
    )(tokens, norm_gain.reshape(1, -1), expert_ids.T, route_weights.T, w_gate, w_up, w_down)


def solution(mesh):
    placed = (
        P(("grp", "ep", "tp"), None),
        P(),
        P(("grp", "ep", "tp"), None),
        P(("grp", "ep", "tp"), None),
        P(None, ("ep", "tp")),
        P(None, ("ep", "tp")),
        P(("ep", "tp"), None),
    )
    return jax.shard_map(
        local, mesh=mesh, in_specs=placed, out_specs=P(("grp", "ep", "tp"), None), check_vma=False
    )
```

time: 99 us -> 90.5 us (0.914)
  Pallas kernels: 94.1 us -> 88.3 us
  local copies, waits for them, and re-layouts: 4.7 us -> 1.88 us
    pallas_call x1, Pallas kernels: 94.1 us -> 88.3 us  [local(): pl.pallas_call(functools.partial(kernel, experts, cap), out_shape=jax.Sha...]
    unnamed x3 -> x1, local copies, waits for them, and re-layouts: 4.7 us -> 1.88 us
where the time goes in v2:
time: 90.5 us; the launch traced here: 90.2 us
  Pallas kernels  88.3 us (98%)
  local copies, waits for them, and re-layouts  1.88 us (2%)
    pallas_call x1, Pallas kernels, local(): pl.pallas_call(functools.partial(kernel, experts, cap), out_shape=jax.Sha...  88.3 us
    unnamed x1, local copies, waits for them, and re-layouts  1.88 us

profile of v2, /device:TPU:9, one launch (start us, length us, event | category | flops | bytes accessed | tf_op | source)
XLA Modules:
  0.0 90.2 jit_solution(1932980102925092580)
XLA Ops:
  0.0 88.3 %shard_map.73 = bf16[128,2048]{1,0:T(8,128)(2,1)} custom-call(bf16[128,2048]{1,0:T(8,128)(2,1)} %tok_ref.1, f32[1,2048]{1,0:T(1,128)} %bitcast.3, s32[2,128]{1,0:T(2,128)} %bitcast.4, f32[2,128]{1,0:T(2,128)} %bitcast.5, bf16[2048,896]{1,0:T(8,128)(2,1)} %gate_ref.1, bf16[2048,896]{1,0:T(8,128)(2,1)} %up_ref.1, bf16[896,2048]{1,0:T(8,128)(2,1)} %down_ref.1), custom_call_target="tpu_custom_call" | custom-call | tf_op jit(solution)/shard_map/pallas_call | solution.py:331
  88.3 1.9 %copy.9 = bf16[128,2048]{1,0:T(8,128)(2,1)} copy(bf16[128,2048]{1,0:T(8,128)(2,1)} %shard_map.73) | data formatting | bytes 1048576
